TPU v7x, 32 devices: a whole 2x2x4 slice. The times are simulated.
32 devices in a mesh: dp: 4 (over y, x), kv: 4 (over z), tp: 2 (over core).
Axes of the slice: x: 2, y: 2, z: 4, core: 2. Of those that a mesh axis runs over, the one named last changes fastest.
Arguments:
- tokens: bfloat16 [128, 4096], P('dp', ('kv', 'tp')), may hold values from -11.5 to 11.5, as said below
- gain_mix: float32 [4096], replicated, may hold values from 0.1 to 1.9
- gain_mlp: float32 [4096], replicated, may hold values from 0.1 to 1.9
- decay_rate: float32 [16], replicated, may hold values from 0.01 to 1
- w_query: bfloat16 [4096, 1024], P('kv', 'tp'), may hold values from -0.09375 to 0.09375
- w_key: bfloat16 [4096, 1024], P('kv', 'tp'), may hold values from -0.09375 to 0.09375
- w_value: bfloat16 [4096, 2048], P('kv', 'tp'), may hold values from -0.09375 to 0.09375
- w_gate: bfloat16 [4096, 2048], P('kv', 'tp'), may hold values from -0.09375 to 0.09375
- w_mix: bfloat16 [2048, 4096], P('tp', 'kv'), may hold values from -0.125 to 0.125
- w_up: bfloat16 [4096, 16384], P(None, ('kv', 'tp')), may hold values from -0.09375 to 0.09375
- w_down: bfloat16 [16384, 4096], P(('kv', 'tp')), may hold values from -0.0625 to 0.0625
- state: float32 [128, 16, 64, 128], P(('dp', 'kv'), 'tp'), may hold values from -2 to 2
Outputs:
- result: bfloat16 [128, 4096], P('dp', ('kv', 'tp'))
- new_state: float32 [128, 16, 64, 128], P(('dp', 'kv'), 'tp')
Inputs may be any that keep to these rules, and one draw needn't show every extreme that they name: `tokens`: feature scales differ across the features.
All inputs are finite; a program needn't handle non-finite values.
Results may differ from a plain program's by a relative error of at most 0.02.
Values may be sent and summed in bfloat16 or wider, within the bound.
A program may use at most 128 MiB of HBM per device.

v0:
```python
import jax
import jax.numpy as jnp
from jax import lax
from jax.sharding import PartitionSpec as P

EPS = 1e-06


def per_device(
    tokens,
    gain_mix,
    gain_mlp,
    decay_rate,
    w_query,
    w_key,
    w_value,
    w_gate,
    w_mix,
    w_up,
    w_down,
    state,
):
    seq_count, head_count, key_width, value_width = state.shape
    both_cols = lax.all_gather(tokens, "tp", axis=1, tiled=True)
    col_count = both_cols.shape[1]
    col_start = lax.axis_index("kv") * col_count
    model_width = col_count * lax.axis_size("kv")
    block_f = both_cols.astype(jnp.float32)
    squares = jnp.sum(block_f * block_f, axis=1)
    row_total = lax.psum(squares, "kv")
    first_scale = lax.rsqrt(row_total / model_width + EPS)
    gain_cols = lax.dynamic_slice_in_dim(gain_mix, col_start, col_count)
    normed = (block_f * first_scale[:, None] * gain_cols[None, :]).astype(jnp.bfloat16)
    own_inputs = lax.psum_scatter(
        jnp.concatenate(
            [
                jnp.dot(normed, weight, preferred_element_type=jnp.float32)
                for weight in (w_query, w_key, w_value, w_gate)
            ],
            axis=1,
        ).astype(jnp.bfloat16),
        "kv",
        scatter_dimension=0,
        tiled=True,
    )
    query_end = head_count * key_width
    key_end = 2 * query_end
    value_end = key_end + head_count * value_width
    query_heads = (
        own_inputs[:, :query_end].astype(jnp.float32).reshape(seq_count, head_count, key_width)
    )
    key_heads = (
        own_inputs[:, query_end:key_end]
        .astype(jnp.float32)
        .reshape(seq_count, head_count, key_width)
    )
    key_heads = key_heads * key_width ** (-0.5)
    value_heads = (
        own_inputs[:, key_end:value_end]
        .astype(jnp.float32)
        .reshape(seq_count, head_count, value_width)
    )
    gate_heads = (
        own_inputs[:, value_end:].astype(jnp.float32).reshape(seq_count, head_count, value_width)
    )
    rates = lax.dynamic_slice_in_dim(decay_rate, lax.axis_index("tp") * head_count, head_count)
    decay = jnp.exp(-rates)[None, :, None, None]
    new_state = decay * state + key_heads[:, :, :, None] * value_heads[:, :, None, :]
    read = jnp.einsum("bhd,bhde->bhe", query_heads, new_state, precision=lax.Precision.HIGHEST)
    read = read * lax.rsqrt(jnp.mean(read * read, axis=2, keepdims=True) + EPS)
    heads_out = (
        (jax.nn.silu(gate_heads) * read)
        .reshape(seq_count, head_count * value_width)
        .astype(jnp.bfloat16)
    )
    partial_value = jnp.dot(
        lax.all_gather(heads_out, "kv", axis=0, tiled=True),
        w_mix,
        preferred_element_type=jnp.float32,
    )
    rounded = lax.optimization_barrier(partial_value.astype(jnp.bfloat16)).astype(jnp.float32)
    mixed = lax.psum_scatter(
        rounded.astype(jnp.bfloat16), "tp", scatter_dimension=1, tiled=True
    ).astype(jnp.float32)
    resid_own = (tokens.astype(jnp.float32) + mixed).astype(jnp.bfloat16)
    rows_full = lax.all_gather(resid_own, ("kv", "tp"), axis=1, tiled=True)
    rows_f = rows_full.astype(jnp.float32)
    second_scale = lax.rsqrt(jnp.mean(rows_f * rows_f, axis=1, keepdims=True) + EPS)
    normed_mlp = (rows_f * second_scale * gain_mlp[None, :]).astype(jnp.bfloat16)
    upper = jnp.dot(normed_mlp, w_up, preferred_element_type=jnp.float32)
    hidden = jnp.square(jax.nn.relu(upper)).astype(jnp.bfloat16)
    summed = lax.psum_scatter(
        jnp.dot(hidden, w_down, preferred_element_type=jnp.float32),
        ("kv", "tp"),
        scatter_dimension=1,
        tiled=True,
    )
    own_width = tokens.shape[1]
    residual_cols = lax.dynamic_slice_in_dim(
        rows_f, lax.axis_index(("kv", "tp")) * own_width, own_width, 1
    )
    result = (residual_cols + summed).astype(jnp.bfloat16)
    return (result, new_state)


def solution(mesh):
    placed = (
        P("dp", ("kv", "tp")),
        P(),
        P(),
        P(),
        P("kv", "tp"),
        P("kv", "tp"),
        P("kv", "tp"),
        P("kv", "tp"),
        P("tp", "kv"),
        P(None, ("kv", "tp")),
        P(("kv", "tp"), None),
        P(("dp", "kv"), "tp", None, None),
    )
    return jax.shard_map(
        per_device,
        mesh=mesh,
        in_specs=placed,
        out_specs=(P("dp", ("kv", "tp")), P(("dp", "kv"), "tp", None, None)),
        check_vma=False,
    )
```

profile of v0, /device:TPU:0, one launch (start us, length us, event | category | flops | bytes accessed | tf_op | source)
XLA Modules:
  0.0 144.6 jit_solution(13502659282743939154)
XLA Ops:
  7.2 0.0 copy-start
  7.2 0.0 reduce-scatter.4.cloned.1.call-start
  7.2 2.3 %all_gather.9 = bf16[32,1024]{1,0:T(8,128)(2,1)S(1)} all-gather(bf16[32,512]{1,0:T(8,128)(2,1)} %param.12), channel_id=1, replica_groups=mesh['dp'=4,'kv'=4,'tp'=2] {'tp'}, dimensions={1}, use_global_device_ids=true | all-gather | bytes 98304 | tf_op jit(solution)/shard_map/all_gather | solution.py:24
  9.6 0.1 fusion.9
  9.7 13.3 %psum.7 = f32[32]{0:T(128)S(1)} all-reduce(f32[32]{0:T(128)S(1)} %fusion.9), channel_id=1, replica_groups=mesh['dp'=4,'kv'=4,'tp'=2] {'kv'}, use_global_device_ids=true, to_apply=%region_1.0 | all-reduce | flops 32 | bytes 256 | tf_op jit(solution)/shard_map/psum | solution.py:30
  23.0 0.7 dynamic_slice.9
  23.7 0.0 copy-start.2
  23.7 1.7 %convolution_convert_fusion.3 = bf16[32,512]{1,0:T(8,128)(2,1)S(1)} fusion(bf16[1024,512]{1,0:T(8,128)(2,1)} %param.17, bf16[32,1024]{1,0:T(8,128)(2,1)S(1)} %all_gather.9, f32[1024]{0:T(1024)S(1)} %dynamic_slice.9, f32[32]{0:T(128)S(1)} %add_rsqrt_fusion.2), kind=kOutput, calls=%fused_computation.7 | convolution fusion | flops 33701888 | bytes 1151104 | tf_op jit(solution)/shard_map/dot_general | solution.py:37
  25.4 1.6 %convolution_convert_fusion.4 = bf16[32,512]{1,0:T(8,128)(2,1)S(1)} fusion(bf16[1024,512]{1,0:T(8,128)(2,1)} %param.16, bf16[32,1024]{1,0:T(8,128)(2,1)S(1)} %all_gather.9, f32[1024]{0:T(1024)S(1)} %dynamic_slice.9, f32[32]{0:T(128)S(1)} %add_rsqrt_fusion.2), kind=kOutput, calls=%fused_computation.8 | convolution fusion | flops 33701888 | bytes 1151104 | tf_op jit(solution)/shard_map/dot_general | solution.py:37
  26.9 0.0 copy-done
  27.0 0.0 copy-start.6
  27.0 0.5 convolution_convert_fusion.2
  27.5 0.0 copy-done.2
  27.5 0.5 convolution_convert_fusion.1
  28.0 0.7 pad_maximum_fusion
  28.7 0.0 reduce-scatter.4.cloned.1.call-update
  28.7 0.0 reduce-scatter.6.cloned.1.call-start
  28.8 0.0 copy-done.6
  28.8 0.1 negate_exponential_fusion
  28.9 17.8 %reduce-scatter.4.cloned.1.call-done = bf16[8,3072]{1,0:T(8,128)(2,1)} async-done(((bf16[32,3072]{1,0:T(8,128)(2,1)}), bf16[8,3072]{1,0:T(8,128)(2,1)}) %reduce-scatter.4.cloned.1.call-update) | async-done | bytes 49168 | tf_op jit(solution)/shard_map/reduce_scatter | solution.py:34
  46.7 0.7 convert_multiply_fusion.3
  47.4 0.1 mul.119
  47.5 0.7 slice.17
  48.2 0.1 reshape.53
  48.3 0.7 fusion.19
  49.0 2.0 %multiply_add_fusion = f32[8,8,64,128]{3,2,1,0:T(8,128)S(1)} fusion(f32[8,8,64,128]{3,2,1,0:T(8,128)} %param.23, f32[8,8,128]{2,1,0:T(8,128)S(1)} %copy.14, f32[8,8,64]{2,1,0:T(8,128)S(1)} %mul.119, f32[8]{0:T(128)S(1)} %negate_exponential_fusion), kind=kLoop, calls=%fused_computation.3 | loop fusion | flops 1572864 | bytes 4243488 | tf_op jit(solution)/shard_map/add | solution.py:68
  51.0 0.0 copy-start.1
  51.0 1.3 copy-done.1
  52.3 0.0 copy-start.4
  52.3 1.1 fusion.26
  53.4 0.0 copy-start.5
  53.4 0.1 fusion.17
  53.5 0.8 fusion.20
  54.3 13.1 %all_gather.10 = bf16[32,1024]{1,0:T(8,128)(2,1)S(1)} all-gather(bf16[8,1024]{1,0:T(8,128)(2,1)S(1)} %fusion.20), channel_id=1, replica_groups=mesh['dp'=4,'kv'=4,'tp'=2] {'kv'}, dimensions={0}, use_global_device_ids=true | all-gather | bytes 81920 | tf_op jit(solution)/shard_map/all_gather | solution.py:77
  67.4 0.0 copy-done.3
  67.4 1.1 convolution_convert_fusion
  68.5 0.0 reduce-scatter.6.cloned.1.call-update
  68.5 0.0 reduce-scatter.8.cloned.1.call-start
  68.6 5.9 %reduce-scatter.6.cloned.1.call-done = bf16[32,512]{1,0:T(8,128)(2,1)} async-done(((bf16[32,1024]{1,0:T(8,128)(2,1)}), bf16[32,512]{1,0:T(8,128)(2,1)}) %reduce-scatter.6.cloned.1.call-update) | async-done | bytes 32784 | tf_op jit(solution)/shard_map/reduce_scatter | solution.py:82
  74.4 0.0 copy-done.4
  74.4 0.8 add_convert_fusion.1
  75.2 14.5 %all_gather.11 = bf16[32,4096]{1,0:T(8,128)(2,1)S(1)} all-gather(bf16[32,512]{1,0:T(8,128)(2,1)S(1)} %add_convert_fusion.1), channel_id=1, replica_groups=mesh['dp'=4,'kv'=4,'tp'=2] {'kv','tp'}, dimensions={1}, use_global_device_ids=true | all-gather | bytes 294912 | tf_op jit(solution)/shard_map/all_gather | solution.py:86
  89.7 0.2 multiply_reduce_fusion
  89.8 0.0 copy-done.5
  89.8 14.4 %fusion.2 = f32[32,4096]{1,0:T(8,128)} fusion(bf16[2048,4096]{1,0:T(8,128)(2,1)} %param.22, bf16[4096,2048]{1,0:T(8,128)(2,1)} %param.21, f32[4096]{0:T(1024)S(1)} %copy-done.5, f32[32]{0:T(128)S(1)} %add_rsqrt_fusion.1, bf16[32,4096]{1,0:T(8,128)(2,1)S(1)} %all_gather.11), kind=kOutput, calls=%fused_computation.9 | convolution fusion | flops 1074462720 | bytes 34357376 | tf_op jit(solution)/shard_map/dot_general | solution.py:93
  104.3 0.0 reduce-scatter.8.cloned.1.call-update
  104.3 32.3 %reduce-scatter.8.cloned.1.call-done = f32[32,512]{1,0:T(8,128)} async-done(((f32[32,4096]{1,0:T(8,128)}), f32[32,512]{1,0:T(8,128)}) %reduce-scatter.8.cloned.1.call-update) | async-done | bytes 65552 | tf_op jit(solution)/shard_map/reduce_scatter | solution.py:92
  136.6 1.5 %add_convert_fusion = bf16[32,512]{1,0:T(8,128)(2,1)} fusion(f32[32,512]{1,0:T(8,128)} %reduce-scatter.8.cloned.1.call-done, f32[32,4096]{1,0:T(8,128)S(1)} %convert_element_type.54, s32[]{:T(128)S(6)} %select_n.11), kind=kLoop, calls=%fused_computation.22 | loop fusion | flops 32768 | bytes 163844 | tf_op jit(solution)/shard_map/convert_element_type | solution.py:102
  (6 shorter events, 0.1 us)
Async XLA Ops:
  7.2 19.8 %copy-start = (bf16[1024,1024]{1,0:T(8,128)(2,1)S(1)}, bf16[1024,1024]{1,0:T(8,128)(2,1)}, u32[]{:S(2)}) copy-start(bf16[1024,1024]{1,0:T(8,128)(2,1)} %param.18) | copy-start | bytes 6291460
  7.2 39.5 %reduce-scatter.4.cloned.1.call-start = ((), (), s32[]{:S(2)}) async-start(), calls=%async_computation.3 | async-start | bytes 245760 | tf_op jit(solution)/shard_map/reduce_scatter | solution.py:34
  23.7 3.8 %copy-start.2 = (bf16[1024,1024]{1,0:T(8,128)(2,1)S(1)}, bf16[1024,1024]{1,0:T(8,128)(2,1)}, u32[]{:S(2)}) copy-start(bf16[1024,1024]{1,0:T(8,128)(2,1)} %param.19) | copy-start | bytes 6291460
  27.0 1.8 %copy-start.6 = (f32[16]{0:T(128)S(1)}, f32[16]{0:T(128)}, u32[]{:S(2)}) copy-start(f32[16]{0:T(128)} %param.15) | copy-start | bytes 196
  28.7 45.7 %reduce-scatter.6.cloned.1.call-start = ((), (), s32[]{:S(2)}) async-start(), calls=%async_computation.4 | async-start | bytes 98304 | tf_op jit(solution)/shard_map/reduce_scatter | solution.py:82
  51.0 1.3 copy-start.1
  52.3 15.1 %copy-start.3 = (bf16[1024,1024]{1,0:T(8,128)(2,1)S(1)}, bf16[1024,1024]{1,0:T(8,128)(2,1)}, u32[]{:S(2)}) copy-start(bf16[1024,1024]{1,0:T(8,128)(2,1)} %param.20) | copy-start | bytes 6291460
  52.3 22.1 %copy-start.4 = (bf16[32,512]{1,0:T(8,128)(2,1)S(1)}, bf16[32,512]{1,0:T(8,128)(2,1)}, u32[]{:S(2)}) copy-start(bf16[32,512]{1,0:T(8,128)(2,1)} %param.12) | copy-start | bytes 98308
  53.4 36.5 %copy-start.5 = (f32[4096]{0:T(1024)S(1)}, f32[4096]{0:T(1024)}, u32[]{:S(2)}) copy-start(f32[4096]{0:T(1024)} %param.14) | copy-start | bytes 49156
  68.5 68.1 %reduce-scatter.8.cloned.1.call-start = ((), (), s32[]{:S(2)}) async-start(), calls=%async_computation.5 | async-start | bytes 589824 | tf_op jit(solution)/shard_map/reduce_scatter | solution.py:92
Sparse Core Ops, SparseCore 0:
  28.8 17.7 reduce-scatter.3
  68.6 5.7 reduce-scatter.5
  104.4 32.1 reduce-scatter.7
where the time goes:
time: 145 us
  waiting for transfers between devices  56 us (39%)
  blocking collectives  43.2 us (30%)
  matrix products  20.9 us (14%)
  between operations  13.8 us (10%)
  other arithmetic  7.63 us (5%)
  local copies, waits for them, and re-layouts  2.92 us (2%)
    reduce_scatter x1, waiting for transfers between devices, per_device(): lax.psum_scatter(jnp.dot(hidden, w_down, preferred_element_type=jnp.float...  32.3 us
    reduce_scatter x1, waiting for transfers between devices, per_device(): lax.psum_scatter(jnp.concatenate([jnp.dot(normed, weight, preferred_eleme...  17.8 us
    all_gather x1, blocking collectives, per_device(): rows_full = lax.all_gather(resid_own, ('kv', 'tp'), axis=1, tiled=True)  14.5 us
    dot_general x1, matrix products, per_device(): jnp.dot(hidden, w_down, preferred_element_type=jnp.float32)  14.4 us
    psum x1, blocking collectives, per_device(): row_total = lax.psum(squares, 'kv')  13.3 us
    all_gather x1, blocking collectives, per_device(): lax.all_gather(heads_out, 'kv', axis=0, tiled=True)  13.1 us
    reduce_scatter x1, waiting for transfers between devices, per_device(): lax.psum_scatter(rounded.astype(jnp.bfloat16), 'tp', scatter_dimension=1,...  5.88 us
    dot_general x4, matrix products, per_device(): jnp.dot(normed, weight, preferred_element_type=jnp.float32)  4.28 us
  transfers between devices with their start and end apart: 3, of which 3 were waited for; matrix products, arithmetic and copies ran while one was open for 0% of the time, Pallas kernels for 0%

commit v1 on v0

--- a/solution.py
+++ b/solution.py
@@ -1,6 +1,9 @@
+import functools
 import jax
 import jax.numpy as jnp
 from jax import lax
+from jax.experimental import pallas as pl
+from jax.experimental.pallas import tpu as pltpu
 from jax.sharding import PartitionSpec as P
 
 EPS = 1e-06
@@ -103,6 +106,442 @@
     return (result, new_state)
 
 
+BF = jnp.bfloat16
+F32 = jnp.float32
+
+
+def layer_kernel(
+    n,
+    tokens_hbm,
+    gain_mix_hbm,
+    gain_mlp_hbm,
+    rate_ref,
+    wq_hbm,
+    wk_hbm,
+    wv_hbm,
+    wg_hbm,
+    wm_hbm,
+    wu_hbm,
+    wd_hbm,
+    state_hbm,
+    result_hbm,
+    new_state_hbm,
+    tok,
+    tok_other,
+    gm,
+    gl,
+    wq,
+    wk,
+    wv,
+    wg,
+    wm,
+    wu,
+    wd,
+    st,
+    part_out,
+    part_in,
+    sq_out,
+    sq_in,
+    own,
+    turned,
+    heads,
+    mix_out,
+    mix_in,
+    resid,
+    upper,
+    pair_out,
+    pair_in,
+    kept,
+    sum_out,
+    sum_in,
+    res,
+    local_sem,
+    up_sem,
+    down_sem,
+    tok_sem,
+    part_send,
+    part_recv,
+    sq_send,
+    sq_recv,
+    head_send,
+    head_recv,
+    mix_sem,
+    res_send,
+    res_recv,
+    fwd_send,
+    pair_send,
+    pair_recv,
+    sum_send,
+    sum_recv,
+):
+    kv = lax.axis_index("kv")
+    tp = lax.axis_index("tp")
+    other = 1 - tp
+    me = 2 * kv + tp
+    rows, width = tok.shape
+    seqs, head_count, dk, dv = st.shape
+    model = 2 * n * width
+    pair_width = 2 * width
+    offsets = sorted(range(1, n), key=lambda o: (min(o, n - o), o))
+
+    def peer(offset):
+        return lax.rem(kv + offset, n)
+
+    def send(src, dst, send_sem, recv_sem, k, t):
+        copy = pltpu.make_async_remote_copy(
+            src_ref=src,
+            dst_ref=dst,
+            send_sem=send_sem,
+            recv_sem=recv_sem,
+            device_id={"kv": k, "tp": t},
+            device_id_type=pl.DeviceIdType.MESH,
+        )
+        copy.start()
+        return copy
+
+    def landed(ref, sem):
+        pltpu.make_async_copy(ref, ref, sem).wait()
+
+    loads = [
+        pltpu.make_async_copy(a, b, local_sem.at[i])
+        for i, (a, b) in enumerate(
+            (
+                (tokens_hbm, tok),
+                (gain_mix_hbm, gm),
+                (wv_hbm, wv),
+                (wg_hbm, wg),
+                (wq_hbm, wq),
+                (wk_hbm, wk),
+                (state_hbm, st),
+                (wm_hbm, wm),
+                (gain_mlp_hbm, gl),
+            )
+        )
+    ]
+    for load in loads:
+        load.start()
+    up_loads = [
+        pltpu.make_async_copy(wu_hbm.at[pl.ds(j * width, width), :], wu.at[j], up_sem.at[j])
+        for j in range(2 * n)
+    ]
+    down_loads = [
+        pltpu.make_async_copy(wd_hbm.at[:, pl.ds(j * width, width)], wd.at[j], down_sem.at[j])
+        for j in range(2 * n)
+    ]
+
+    barrier = pltpu.get_barrier_semaphore()
+    for offset in range(n):
+        for t in (tp, other) if offset else (other,):
+            pl.semaphore_signal(
+                barrier,
+                inc=1,
+                device_id={"kv": peer(offset), "tp": t},
+                device_id_type=pl.DeviceIdType.MESH,
+            )
+    pl.semaphore_wait(barrier, 2 * n - 1)
+
+    loads[0].wait()
+    tok_copy = send(tok, tok_other, tok_sem.at[0], tok_sem.at[1], kv, other)
+    loads[1].wait()
+    tok_copy.wait_recv()
+    mine = tok[...].astype(F32)
+    theirs = tok_other[...].astype(F32)
+    first = tp == 0
+    left = jnp.where(first, mine, theirs)
+    right = jnp.where(first, theirs, mine)
+    both = jnp.concatenate([left, right], axis=1)
+    squares = jnp.sum(both * both, axis=1, keepdims=True)
+    scaled = (both * gm[:, pl.ds(pl.multiple_of(kv * pair_width, 128), pair_width)]).astype(BF)
+    squares = jnp.broadcast_to(squares, (rows, 128))
+    for k in range(n):
+        sq_out[k] = squares[k * seqs : (k + 1) * seqs]
+    q_width, v_width = wq.shape[1], wv.shape[1]
+    starts = (2 * q_width, 2 * q_width + v_width, 0, q_width)
+    for index, weight in enumerate((wv, wg, wq, wk)):
+        loads[2 + index].wait()
+        product = jnp.dot(scaled, weight[...], preferred_element_type=F32)
+        cols = slice(starts[index], starts[index] + weight.shape[1])
+        for k in range(n):
+            part_out[k, :, cols] = product[k * seqs : (k + 1) * seqs].astype(BF)
+    sent = []
+    for offset in reversed(offsets):
+        k = peer(offset)
+        sent.append(send(sq_out.at[k], sq_in.at[kv], sq_send.at[offset], sq_recv.at[kv], k, tp))
+        sent.append(
+            send(part_out.at[k], part_in.at[kv], part_send.at[offset], part_recv.at[kv], k, tp)
+        )
+    for load in up_loads + down_loads:
+        load.start()
+    total = part_out[kv].astype(F32)
+    sq_total = sq_out[kv]
+    for offset in offsets:
+        k = peer(offset)
+        landed(sq_in.at[k], sq_recv.at[k])
+        landed(part_in.at[k], part_recv.at[k])
+        total += part_in[k].astype(F32)
+        sq_total += sq_in[k]
+    total = total * lax.rsqrt(sq_total / model + EPS)[:, :1]
+    own[...] = total
+    blank = jnp.zeros((128 - 2 * seqs, q_width), F32)
+    turned[...] = jnp.concatenate(
+        [total[:, :q_width], total[:, q_width : 2 * q_width] * dk ** (-0.5), blank], axis=0
+    ).T
+    loads[6].wait()
+
+    def one_head(h, carry):
+        cols = turned[pl.ds(pl.multiple_of(h * dk, dk), dk), :]
+        value = own[:, pl.ds(pl.multiple_of(2 * q_width + h * dv, 128), dv)]
+        gate = own[:, pl.ds(pl.multiple_of(2 * q_width + v_width + h * dv, 128), dv)]
+        decay = jnp.exp(jnp.full((1, dv), -rate_ref[tp * head_count + h], F32))
+        reads = []
+        for b in range(seqs):
+            new = decay * st[b, h] + cols[:, seqs + b : seqs + b + 1] * value[b : b + 1]
+            st[b, h] = new
+            reads.append(jnp.sum(cols[:, b : b + 1] * new, axis=0, keepdims=True))
+        read = jnp.concatenate(reads, axis=0)
+        read = read * lax.rsqrt(jnp.mean(read * read, axis=1, keepdims=True) + EPS)
+        out = gate / (1.0 + jnp.exp(-gate)) * read
+        heads[kv, :, pl.ds(pl.multiple_of(h * dv, 128), dv)] = out.astype(BF)
+        return carry
+
+    lax.fori_loop(0, head_count, one_head, 0)
+    for offset in reversed(offsets):
+        sent.append(
+            send(heads.at[kv], heads.at[kv], head_send.at[offset], head_recv.at[kv], peer(offset), tp)
+        )
+    state_copy = pltpu.make_async_copy(st, new_state_hbm, local_sem.at[9])
+    state_copy.start()
+    loads[7].wait()
+    for offset in offsets:
+        k = peer(offset)
+        landed(heads.at[k], head_recv.at[k])
+    gathered = jnp.concatenate([heads[k].astype(F32) for k in range(n)], axis=0).astype(BF)
+    mix_out[...] = jnp.dot(
+        gathered,
+        wm[:, pl.ds(pl.multiple_of(other * width, 128), width)],
+        preferred_element_type=F32,
+    ).astype(BF)
+    mix_copy = send(mix_out, mix_in, mix_sem.at[0], mix_sem.at[1], kv, other)
+    own_mix = jnp.dot(
+        gathered,
+        wm[:, pl.ds(pl.multiple_of(tp * width, 128), width)],
+        preferred_element_type=F32,
+    ).astype(BF)
+    mix_copy.wait_recv()
+    resid[me] = (
+        tok[...].astype(F32) + (own_mix.astype(F32) + mix_in[...].astype(F32))
+    ).astype(BF)
+    for offset in reversed(offsets):
+        sent.append(
+            send(resid.at[me], resid.at[me], res_send.at[offset], res_recv.at[me], peer(offset), tp)
+        )
+    sent.append(send(resid.at[me], resid.at[me], res_send.at[0], res_recv.at[me], kv, other))
+    loads[8].wait()
+
+    def up_step(j, so_far):
+        pltpu.make_async_copy(
+            wu_hbm.at[pl.ds(0, width), :], wu.at[j], up_sem.at[j]
+        ).wait()
+        block = resid[j].astype(F32)
+        cols = pl.ds(pl.multiple_of(j * width, 128), width)
+        product = jnp.dot((block * gl[:, cols]).astype(BF), wu[j], preferred_element_type=F32)
+        squares = jnp.sum(block * block, axis=1, keepdims=True)
+        if so_far is None:
+            upper[...] = product
+            return squares
+        upper[...] += product
+        return so_far + squares
+
+    def direct(offset, so_far):
+        j = 2 * peer(offset) + tp
+        landed(resid.at[j], res_recv.at[j])
+        sent.append(send(resid.at[j], resid.at[j], fwd_send.at[offset], res_recv.at[j], kv, other))
+        return up_step(j, so_far)
+
+    def passed(offset, so_far):
+        j = 2 * peer(offset) + other
+        landed(resid.at[j], res_recv.at[j])
+        return up_step(j, so_far)
+
+    row_sq = up_step(me, None)
+    row_sq = passed(0, row_sq)
+    waiting = []
+    for offset in offsets:
+        row_sq = direct(offset, row_sq)
+        waiting.append(offset)
+        if len(waiting) > 1:
+            row_sq = passed(waiting.pop(0), row_sq)
+    for offset in waiting:
+        row_sq = passed(offset, row_sq)
+    positive = jnp.maximum(upper[...] * lax.rsqrt(row_sq / model + EPS), 0.0)
+    hidden = (positive * positive).astype(BF)
+
+    def down_dot(j):
+        pltpu.make_async_copy(
+            wd_hbm.at[:, pl.ds(0, width)], wd.at[j], down_sem.at[j]
+        ).wait()
+        return jnp.dot(hidden, wd[j], preferred_element_type=F32)
+
+    def combine(offset):
+        k = peer(offset)
+        landed(pair_in.at[k], pair_recv.at[k])
+        sum_out[k] = (kept[k] + pair_in[k].astype(F32)).astype(BF)
+        sent.append(send(sum_out.at[k], sum_in.at[kv], sum_send.at[offset], sum_recv.at[kv], k, tp))
+
+    pending = None
+    for offset in offsets[::-1] + [0]:
+        k = peer(offset)
+        pair_out[k] = down_dot(2 * k + other).astype(BF)
+        sent.append(
+            send(pair_out.at[k], pair_in.at[k], pair_send.at[k], pair_recv.at[k], kv, other)
+        )
+        if pending is not None:
+            combine(pending)
+        kept[k] = down_dot(2 * k + tp)
+        pending = offset
+    final = resid[me].astype(F32) + kept[kv]
+    landed(pair_in.at[kv], pair_recv.at[kv])
+    final += pair_in[kv].astype(F32)
+    for offset in offsets:
+        k = peer(offset)
+        landed(sum_in.at[k], sum_recv.at[k])
+        final += sum_in[k].astype(F32)
+    res[...] = final.astype(BF)
+    out_copy = pltpu.make_async_copy(res, result_hbm, local_sem.at[10])
+    out_copy.start()
+    tok_copy.wait_send()
+    mix_copy.wait_send()
+    for copy in sent:
+        copy.wait_send()
+    state_copy.wait()
+    out_copy.wait()
+
+
+def fused_device(
+    n,
+    tokens,
+    gain_mix,
+    gain_mlp,
+    decay_rate,
+    w_query,
+    w_key,
+    w_value,
+    w_gate,
+    w_mix,
+    w_up,
+    w_down,
+    state,
+):
+    rows, width = tokens.shape
+    seqs, head_count, dk, dv = state.shape
+    model = gain_mix.shape[0]
+    qk_width, v_width = w_query.shape[1], w_value.shape[1]
+    all_width = 2 * qk_width + 2 * v_width
+    units = w_up.shape[1]
+    anywhere = pl.BlockSpec(memory_space=pl.ANY)
+    dma = pltpu.SemaphoreType.DMA
+    vmem = pltpu.VMEM
+    scratch = [
+        vmem((rows, width), BF),
+        vmem((rows, width), BF),
+        vmem((1, model), F32),
+        vmem((1, model), F32),
+        vmem(w_query.shape, BF),
+        vmem(w_key.shape, BF),
+        vmem(w_value.shape, BF),
+        vmem(w_gate.shape, BF),
+        vmem(w_mix.shape, BF),
+        vmem((2 * n, width, units), BF),
+        vmem((2 * n, units, width), BF),
+        vmem(state.shape, F32),
+        vmem((n, seqs, all_width), BF),
+        vmem((n, seqs, all_width), BF),
+        vmem((n, seqs, 128), F32),
+        vmem((n, seqs, 128), F32),
+        vmem((seqs, all_width), F32),
+        vmem((qk_width, 128), F32),
+        vmem((n, seqs, v_width), BF),
+        vmem((rows, width), BF),
+        vmem((rows, width), BF),
+        vmem((2 * n, rows, width), BF),
+        vmem((rows, units), F32),
+        vmem((n, rows, width), BF),
+        vmem((n, rows, width), BF),
+        vmem((n, rows, width), F32),
+        vmem((n, rows, width), BF),
+        vmem((n, rows, width), BF),
+        vmem((rows, width), BF),
+        dma((11,)),
+        dma((2 * n,)),
+        dma((2 * n,)),
+        dma((2,)),
+        dma((n,)),
+        dma((n,)),
+        dma((n,)),
+        dma((n,)),
+        dma((n,)),
+        dma((n,)),
+        dma((2,)),
+        dma((n,)),
+        dma((2 * n,)),
+        dma((n,)),
+        dma((n,)),
+        dma((n,)),
+        dma((n,)),
+        dma((n,)),
+    ]
+    return pl.pallas_call(
+        functools.partial(layer_kernel, n),
+        out_shape=(
+            jax.ShapeDtypeStruct(tokens.shape, tokens.dtype),
+            jax.ShapeDtypeStruct(state.shape, state.dtype),
+        ),
+        in_specs=[anywhere] * 3
+        + [pl.BlockSpec(memory_space=pltpu.SMEM)]
+        + [anywhere] * 8,
+        out_specs=(anywhere, anywhere),
+        scratch_shapes=scratch,
+        compiler_params=pltpu.CompilerParams(
+            collective_id=0, has_side_effects=True, vmem_limit_bytes=60 * 1024 * 1024
+        ),
+        name="retention_layer",
+    )(
+        tokens,
+        gain_mix.reshape(1, model),
+        gain_mlp.reshape(1, model),
+        decay_rate,
+        w_query,
+        w_key,
+        w_value,
+        w_gate,
+        w_mix,
+        w_up,
+        w_down,
+        state,
+    )
+
+
+def device_program(n, n_tp, tokens, *rest):
+    state = rest[-1]
+    rows, width = tokens.shape
+    seqs, head_count, dk, dv = state.shape
+    w_query, w_up = rest[3], rest[8]
+    weight_bytes = 2 * sum(weight.size for weight in rest[3:-1])
+    fits = weight_bytes + 4 * state.size <= 48 * 1024 * 1024
+    aligned = (
+        width % 128 == 0
+        and dv % 128 == 0
+        and w_query.shape[1] % 128 == 0
+        and w_up.shape[1] % 128 == 0
+        and dk % 8 == 0
+        and seqs % 8 == 0
+        and 2 * seqs <= 128
+    )
+    if n_tp == 2 and fits and aligned:
+        return fused_device(n, tokens, *rest)
+    return per_device(tokens, *rest)
+
+
 def solution(mesh):
     placed = (
         P("dp", ("kv", "tp")),
@@ -119,7 +558,7 @@
         P(("dp", "kv"), "tp", None, None),
     )
     return jax.shard_map(
-        per_device,
+        functools.partial(device_program, mesh.shape["kv"], mesh.shape["tp"]),
         mesh=mesh,
         in_specs=placed,
         out_specs=(P("dp", ("kv", "tp")), P(("dp", "kv"), "tp", None, None)),

time: 145 us -> 43.2 us (0.30)
  waiting for transfers between devices: 56 us -> 0 us
  blocking collectives: 43.2 us -> 0 us
  Pallas kernels: 0 us -> 37.8 us
  matrix products: 20.9 us -> 0 us
  between operations: 13.8 us -> 0.64 us
  other arithmetic: 7.63 us -> 0 us
  local copies, waits for them, and re-layouts: 2.92 us -> 4.53 us
    reduce_scatter x3 -> x0, waiting for transfers between devices: 56 us -> none  [the longest x1 32.3 us: per_device(): lax.psum_scatter(jnp.dot(hidden, w_down, preferred_element_type=jnp.float...]
    pallas_call x0 -> x1, Pallas kernels: none -> 37.8 us  [fused_device(): pl.pallas_call(functools.partial(layer_kernel, n), out_shape=(jax.ShapeDt...]
    all_gather x3 -> x0, blocking collectives: 29.9 us -> none  [the longest x1 14.5 us: per_device(): rows_full = lax.all_gather(resid_own, ('kv', 'tp'), axis=1, tiled=True)]
    dot_general x7 -> x0, matrix products: 20.9 us -> none  [the longest x1 14.4 us: per_device(): jnp.dot(hidden, w_down, preferred_element_type=jnp.float32)]
    psum x1 -> x0, blocking collectives: 13.3 us -> none  [per_device(): row_total = lax.psum(squares, 'kv')]
    unnamed x14 -> x2, local copies, waits for them, and re-layouts: 1.35 us -> 4.53 us
    convert_element_type x4 -> x0, other arithmetic: 3.07 us -> none  [the longest x1 1.46 us: per_device(): result = (residual_cols + summed).astype(jnp.bfloat16)]
    add x1 -> x0, other arithmetic: 1.96 us -> none  [per_device(): decay * state + key_heads[:, :, :, None] * value_heads[:, :, None, :]]
  transfers between devices with their start and end apart: 3 -> 0, of which waited for: 3 -> 0; matrix products, arithmetic and copies ran while one was open for 0% -> 0% of each run, Pallas kernels for 0% -> 0%
where the time goes in v1:
time: 43.2 us; the launch traced here: 43 us
  Pallas kernels  37.8 us (87%)
  local copies, waits for them, and re-layouts  4.53 us (10%)
  between operations  0.64 us (1%)
    pallas_call x1, Pallas kernels, fused_device(): pl.pallas_call(functools.partial(layer_kernel, n), out_shape=(jax.ShapeDt...  37.8 us
    unnamed x2, local copies, waits for them, and re-layouts  4.53 us

profile of v1, /device:TPU:0, one launch (start us, length us, event | category | flops | bytes accessed | tf_op | source)
XLA Modules:
  0.0 43.0 jit_solution(8288062828114946465)
XLA Ops:
  0.6 37.8 %retention_layer.1 = (bf16[32,512]{1,0:T(8,128)(2,1)}, f32[8,8,64,128]{3,2,1,0:T(8,128)}) custom-call(bf16[32,512]{1,0:T(8,128)(2,1)} %tokens_hbm.1, f32[1,4096]{1,0:T(1,128)} %bitcast.2, f32[1,4096]{1,0:T(1,128)} %bitcast.3, f32[16]{0:T(128)} %rate_ref.1, bf16[1024,512]{1,0:T(8,128)(2,1)} %wq_hbm.1, bf16[1024,512]{1,0:T(8,128)(2,1)} %wk_hbm.1, ...), custom_call_target="tpu_custom_call" | custom-call | tf_op jit(solution)/shard_map/retention_layer/pallas_call | solution.py:493
  38.4 1.4 %copy.16 = bf16[32,512]{1,0:T(8,128)(2,1)} copy(bf16[32,512]{1,0:T(8,128)(2,1)} %get-tuple-element.4) | data formatting | bytes 65536
  39.8 3.2 %copy.17 = f32[8,8,64,128]{3,2,1,0:T(8,128)} copy(f32[8,8,64,128]{3,2,1,0:T(8,128)} %get-tuple-element.5) | data formatting | bytes 4194304

commit v2 on v1

--- a/solution.py
+++ b/solution.py
@@ -124,8 +124,8 @@
     wu_hbm,
     wd_hbm,
     state_hbm,
-    result_hbm,
-    new_state_hbm,
+    res,
+    st,
     tok,
     tok_other,
     gm,
@@ -137,12 +137,17 @@
     wm,
     wu,
     wd,
-    st,
-    part_out,
-    part_in,
+    half_done,
+    qk_out,
+    qk_in,
+    v_out,
+    v_in,
+    g_out,
+    g_in,
     sq_out,
     sq_in,
-    own,
+    own_v,
+    own_read,
     turned,
     heads,
     mix_out,
@@ -154,7 +159,6 @@
     kept,
     sum_out,
     sum_in,
-    res,
     local_sem,
     up_sem,
     down_sem,
@@ -182,10 +186,16 @@
     seqs, head_count, dk, dv = st.shape
     model = 2 * n * width
     pair_width = 2 * width
-    offsets = sorted(range(1, n), key=lambda o: (min(o, n - o), o))
-
-    def peer(offset):
-        return lax.rem(kv + offset, n)
+    upper_half = kv // (n // 2)
+
+    def far_peer(i):
+        after = 1 - (kv - i - 1 + n) // n
+        above = 1 - (kv - (n - 1 - i) + n) // n
+        from_top = n - 2 - i + above
+        return (1 - upper_half) * from_top + upper_half * (i + after)
+
+    far = [far_peer(i) for i in range(n - 1)]
+    near = far[::-1]
 
     def send(src, dst, send_sem, recv_sem, k, t):
         copy = pltpu.make_async_remote_copy(
@@ -208,10 +218,10 @@
             (
                 (tokens_hbm, tok),
                 (gain_mix_hbm, gm),
+                (wq_hbm, wq),
+                (wk_hbm, wk),
                 (wv_hbm, wv),
                 (wg_hbm, wg),
-                (wq_hbm, wq),
-                (wk_hbm, wk),
                 (state_hbm, st),
                 (wm_hbm, wm),
                 (gain_mlp_hbm, gl),
@@ -230,12 +240,12 @@
     ]
 
     barrier = pltpu.get_barrier_semaphore()
-    for offset in range(n):
-        for t in (tp, other) if offset else (other,):
+    for k in far + [kv]:
+        for t in (other,) if k is kv else (other, tp):
             pl.semaphore_signal(
                 barrier,
                 inc=1,
-                device_id={"kv": peer(offset), "tp": t},
+                device_id={"kv": k, "tp": t},
                 device_id_type=pl.DeviceIdType.MESH,
             )
     pl.semaphore_wait(barrier, 2 * n - 1)
@@ -243,77 +253,122 @@
     loads[0].wait()
     tok_copy = send(tok, tok_other, tok_sem.at[0], tok_sem.at[1], kv, other)
     loads[1].wait()
+
+    def half_of(half, block):
+        cols = pl.ds(pl.multiple_of(kv * pair_width + half * width, 128), width)
+        values = block[...].astype(F32)
+        return (values * gm[:, cols]).astype(BF), jnp.sum(values * values, axis=1, keepdims=True)
+
+    q_width, v_width = wq.shape[1], wv.shape[1]
+    k_at, v_at, g_at = q_width, 2 * q_width, 2 * q_width + v_width
+    weights = ((wq, 0, loads[2]), (wk, k_at, loads[3]), (wv, v_at, loads[4]), (wg, g_at, loads[5]))
+    scaled, own_squares = half_of(tp, tok)
+    own_rows = pl.ds(pl.multiple_of(tp * width, 128), width)
+    for weight, start, load in weights:
+        load.wait()
+        product = jnp.dot(scaled, weight[own_rows, :], preferred_element_type=F32)
+        half_done[:, start : start + weight.shape[1]] = product
     tok_copy.wait_recv()
-    mine = tok[...].astype(F32)
-    theirs = tok_other[...].astype(F32)
-    first = tp == 0
-    left = jnp.where(first, mine, theirs)
-    right = jnp.where(first, theirs, mine)
-    both = jnp.concatenate([left, right], axis=1)
-    squares = jnp.sum(both * both, axis=1, keepdims=True)
-    scaled = (both * gm[:, pl.ds(pl.multiple_of(kv * pair_width, 128), pair_width)]).astype(BF)
-    squares = jnp.broadcast_to(squares, (rows, 128))
+    scaled, squares = half_of(other, tok_other)
+    squares = jnp.broadcast_to(squares + own_squares, (rows, 128))
     for k in range(n):
         sq_out[k] = squares[k * seqs : (k + 1) * seqs]
-    q_width, v_width = wq.shape[1], wv.shape[1]
-    starts = (2 * q_width, 2 * q_width + v_width, 0, q_width)
-    for index, weight in enumerate((wv, wg, wq, wk)):
-        loads[2 + index].wait()
-        product = jnp.dot(scaled, weight[...], preferred_element_type=F32)
-        cols = slice(starts[index], starts[index] + weight.shape[1])
+    sent = []
+    for i, k in enumerate(far):
+        sent.append(send(sq_out.at[k], sq_in.at[kv], sq_send.at[i], sq_recv.at[kv], k, tp))
+    other_rows = pl.ds(pl.multiple_of(other * width, 128), width)
+    parts = ((qk_out, qk_in), (v_out, v_in), (g_out, g_in))
+
+    def finish(weight, start, part, at):
+        product = jnp.dot(scaled, weight[other_rows, :], preferred_element_type=F32)
+        product += half_done[:, start : start + weight.shape[1]]
         for k in range(n):
-            part_out[k, :, cols] = product[k * seqs : (k + 1) * seqs].astype(BF)
-    sent = []
-    for offset in reversed(offsets):
-        k = peer(offset)
-        sent.append(send(sq_out.at[k], sq_in.at[kv], sq_send.at[offset], sq_recv.at[kv], k, tp))
-        sent.append(
-            send(part_out.at[k], part_in.at[kv], part_send.at[offset], part_recv.at[kv], k, tp)
-        )
+            parts[part][0][k, :, at : at + weight.shape[1]] = product[
+                k * seqs : (k + 1) * seqs
+            ].astype(BF)
+
+    def scatter(part):
+        source, target = parts[part]
+        for i, k in enumerate(far):
+            sent.append(
+                send(
+                    source.at[k],
+                    target.at[kv],
+                    part_send.at[part, i],
+                    part_recv.at[part, kv],
+                    k,
+                    tp,
+                )
+            )
+
+    def collect(part):
+        source, target = parts[part]
+        total = source[kv].astype(F32)
+        for k in near:
+            landed(target.at[k], part_recv.at[part, k])
+            total += target[k].astype(F32)
+        return total * first_scale
+
+    finish(wq, 0, 0, 0)
+    finish(wk, k_at, 0, q_width)
+    scatter(0)
+    finish(wv, v_at, 1, 0)
+    scatter(1)
+    finish(wg, g_at, 2, 0)
+    scatter(2)
     for load in up_loads + down_loads:
         load.start()
-    total = part_out[kv].astype(F32)
     sq_total = sq_out[kv]
-    for offset in offsets:
-        k = peer(offset)
+    for k in near:
         landed(sq_in.at[k], sq_recv.at[k])
-        landed(part_in.at[k], part_recv.at[k])
-        total += part_in[k].astype(F32)
         sq_total += sq_in[k]
-    total = total * lax.rsqrt(sq_total / model + EPS)[:, :1]
-    own[...] = total
+    first_scale = lax.rsqrt(sq_total / model + EPS)[:, :1]
+    both = collect(0)
     blank = jnp.zeros((128 - 2 * seqs, q_width), F32)
-    turned[...] = jnp.concatenate(
-        [total[:, :q_width], total[:, q_width : 2 * q_width] * dk ** (-0.5), blank], axis=0
-    ).T
+    turned[...] = (
+        jnp.concatenate([both[:, :q_width], both[:, q_width:] * dk ** (-0.5), blank], axis=0)
+        .T.astype(BF)
+        .astype(F32)
+    )
+    own_v[...] = collect(1)
     loads[6].wait()
 
-    def one_head(h, carry):
-        cols = turned[pl.ds(pl.multiple_of(h * dk, dk), dk), :]
-        value = own[:, pl.ds(pl.multiple_of(2 * q_width + h * dv, 128), dv)]
-        gate = own[:, pl.ds(pl.multiple_of(2 * q_width + v_width + h * dv, 128), dv)]
+    lane = lax.broadcasted_iota(jnp.int32, (dk, 128), 1)
+    ones = jnp.ones((128, dv), BF)
+    above = jnp.zeros((seqs, dv), F32)
+    below = jnp.zeros((128 - 2 * seqs, dv), F32)
+
+    def one_head(h):
+        cols = turned[h * dk : (h + 1) * dk, :]
+        value = own_v[:, h * dv : (h + 1) * dv]
+        value = jnp.concatenate([above, value, below], axis=0).astype(BF)
+
+        def picked(first):
+            return jnp.concatenate(
+                [jnp.where(lane == first + b, cols, 0.0) for b in range(seqs)], axis=0
+            ).astype(BF)
+
+        outer = jnp.dot(picked(seqs), value, preferred_element_type=F32)
+        query = jnp.dot(picked(0), ones, preferred_element_type=F32)
         decay = jnp.exp(jnp.full((1, dv), -rate_ref[tp * head_count + h], F32))
         reads = []
         for b in range(seqs):
-            new = decay * st[b, h] + cols[:, seqs + b : seqs + b + 1] * value[b : b + 1]
+            new = decay * st[b, h] + outer[b * dk : (b + 1) * dk]
             st[b, h] = new
-            reads.append(jnp.sum(cols[:, b : b + 1] * new, axis=0, keepdims=True))
+            reads.append(jnp.sum(query[b * dk : (b + 1) * dk] * new, axis=0, keepdims=True))
         read = jnp.concatenate(reads, axis=0)
-        read = read * lax.rsqrt(jnp.mean(read * read, axis=1, keepdims=True) + EPS)
-        out = gate / (1.0 + jnp.exp(-gate)) * read
-        heads[kv, :, pl.ds(pl.multiple_of(h * dv, 128), dv)] = out.astype(BF)
-        return carry
-
-    lax.fori_loop(0, head_count, one_head, 0)
-    for offset in reversed(offsets):
-        sent.append(
-            send(heads.at[kv], heads.at[kv], head_send.at[offset], head_recv.at[kv], peer(offset), tp)
+        own_read[:, h * dv : (h + 1) * dv] = read * lax.rsqrt(
+            jnp.mean(read * read, axis=1, keepdims=True) + EPS
         )
-    state_copy = pltpu.make_async_copy(st, new_state_hbm, local_sem.at[9])
-    state_copy.start()
+
+    for h in range(head_count):
+        one_head(h)
+    gate = collect(2)
+    heads[kv] = (gate / (1.0 + jnp.exp(-gate)) * own_read[...]).astype(BF)
+    for i, k in enumerate(far):
+        sent.append(send(heads.at[kv], heads.at[kv], head_send.at[i], head_recv.at[kv], k, tp))
     loads[7].wait()
-    for offset in offsets:
-        k = peer(offset)
+    for k in near:
         landed(heads.at[k], head_recv.at[k])
     gathered = jnp.concatenate([heads[k].astype(F32) for k in range(n)], axis=0).astype(BF)
     mix_out[...] = jnp.dot(
@@ -331,11 +386,9 @@
     resid[me] = (
         tok[...].astype(F32) + (own_mix.astype(F32) + mix_in[...].astype(F32))
     ).astype(BF)
-    for offset in reversed(offsets):
-        sent.append(
-            send(resid.at[me], resid.at[me], res_send.at[offset], res_recv.at[me], peer(offset), tp)
-        )
-    sent.append(send(resid.at[me], resid.at[me], res_send.at[0], res_recv.at[me], kv, other))
+    for i, k in enumerate(far):
+        sent.append(send(resid.at[me], resid.at[me], res_send.at[i], res_recv.at[me], k, tp))
+    sent.append(send(resid.at[me], resid.at[me], res_send.at[n - 1], res_recv.at[me], kv, other))
     loads[8].wait()
 
     def up_step(j, so_far):
@@ -352,27 +405,25 @@
         upper[...] += product
         return so_far + squares
 
-    def direct(offset, so_far):
-        j = 2 * peer(offset) + tp
+    def direct(i, so_far):
+        j = 2 * near[i] + tp
         landed(resid.at[j], res_recv.at[j])
-        sent.append(send(resid.at[j], resid.at[j], fwd_send.at[offset], res_recv.at[j], kv, other))
+        sent.append(send(resid.at[j], resid.at[j], fwd_send.at[i], res_recv.at[j], kv, other))
         return up_step(j, so_far)
 
-    def passed(offset, so_far):
-        j = 2 * peer(offset) + other
+    def passed(k, so_far):
+        j = 2 * k + other
         landed(resid.at[j], res_recv.at[j])
         return up_step(j, so_far)
 
     row_sq = up_step(me, None)
-    row_sq = passed(0, row_sq)
-    waiting = []
-    for offset in offsets:
-        row_sq = direct(offset, row_sq)
-        waiting.append(offset)
-        if len(waiting) > 1:
-            row_sq = passed(waiting.pop(0), row_sq)
-    for offset in waiting:
-        row_sq = passed(offset, row_sq)
+    row_sq = passed(kv, row_sq)
+    for i in range(n - 1):
+        row_sq = direct(i, row_sq)
+        if i > 0:
+            row_sq = passed(near[i - 1], row_sq)
+    if n > 1:
+        row_sq = passed(near[-1], row_sq)
     positive = jnp.maximum(upper[...] * lax.rsqrt(row_sq / model + EPS), 0.0)
     hidden = (positive * positive).astype(BF)
 
@@ -382,39 +433,48 @@
         ).wait()
         return jnp.dot(hidden, wd[j], preferred_element_type=F32)
 
-    def combine(offset):
-        k = peer(offset)
-        landed(pair_in.at[k], pair_recv.at[k])
-        sum_out[k] = (kept[k] + pair_in[k].astype(F32)).astype(BF)
-        sent.append(send(sum_out.at[k], sum_in.at[kv], sum_send.at[offset], sum_recv.at[kv], k, tp))
-
-    pending = None
-    for offset in offsets[::-1] + [0]:
-        k = peer(offset)
+    def for_other(k):
         pair_out[k] = down_dot(2 * k + other).astype(BF)
         sent.append(
             send(pair_out.at[k], pair_in.at[k], pair_send.at[k], pair_recv.at[k], kv, other)
         )
-        if pending is not None:
-            combine(pending)
+
+    def combine(i):
+        k = far[i]
         kept[k] = down_dot(2 * k + tp)
-        pending = offset
+        landed(pair_in.at[k], pair_recv.at[k])
+        sum_out[k] = (kept[k] + pair_in[k].astype(F32)).astype(BF)
+        sent.append(send(sum_out.at[k], sum_in.at[kv], sum_send.at[i], sum_recv.at[kv], k, tp))
+
+    for_other(far[0])
+    for i in range(n - 1):
+        if i < n - 2:
+            for_other(far[i + 1])
+        combine(i)
+    for_other(kv)
+    kept[kv] = down_dot(2 * kv + tp)
     final = resid[me].astype(F32) + kept[kv]
     landed(pair_in.at[kv], pair_recv.at[kv])
     final += pair_in[kv].astype(F32)
-    for offset in offsets:
-        k = peer(offset)
+    for k in near:
         landed(sum_in.at[k], sum_recv.at[k])
         final += sum_in[k].astype(F32)
     res[...] = final.astype(BF)
-    out_copy = pltpu.make_async_copy(res, result_hbm, local_sem.at[10])
-    out_copy.start()
     tok_copy.wait_send()
     mix_copy.wait_send()
     for copy in sent:
         copy.wait_send()
-    state_copy.wait()
-    out_copy.wait()
+
+
+def write_out(res, st, result_hbm, state_hbm, sems):
+    copies = [
+        pltpu.make_async_copy(st, state_hbm, sems.at[0]),
+        pltpu.make_async_copy(res, result_hbm, sems.at[1]),
+    ]
+    for copy in copies:
+        copy.start()
+    for copy in copies:
+        copy.wait()
 
 
 def fused_device(
@@ -438,7 +498,8 @@
     qk_width, v_width = w_query.shape[1], w_value.shape[1]
     all_width = 2 * qk_width + 2 * v_width
     units = w_up.shape[1]
-    anywhere = pl.BlockSpec(memory_space=pl.ANY)
+    anywhere = pl.BlockSpec(memory_space=pltpu.HBM)
+    inside = pl.BlockSpec(memory_space=pltpu.VMEM)
     dma = pltpu.SemaphoreType.DMA
     vmem = pltpu.VMEM
     scratch = [
@@ -453,12 +514,17 @@
         vmem(w_mix.shape, BF),
         vmem((2 * n, width, units), BF),
         vmem((2 * n, units, width), BF),
-        vmem(state.shape, F32),
-        vmem((n, seqs, all_width), BF),
-        vmem((n, seqs, all_width), BF),
+        vmem((rows, all_width), F32),
+        vmem((n, seqs, 2 * qk_width), BF),
+        vmem((n, seqs, 2 * qk_width), BF),
+        vmem((n, seqs, v_width), BF),
+        vmem((n, seqs, v_width), BF),
+        vmem((n, seqs, v_width), BF),
+        vmem((n, seqs, v_width), BF),
         vmem((n, seqs, 128), F32),
         vmem((n, seqs, 128), F32),
-        vmem((seqs, all_width), F32),
+        vmem((seqs, v_width), F32),
+        vmem((seqs, v_width), F32),
         vmem((qk_width, 128), F32),
         vmem((n, seqs, v_width), BF),
         vmem((rows, width), BF),
@@ -470,13 +536,12 @@
         vmem((n, rows, width), F32),
         vmem((n, rows, width), BF),
         vmem((n, rows, width), BF),
-        vmem((rows, width), BF),
-        dma((11,)),
+        dma((9,)),
         dma((2 * n,)),
         dma((2 * n,)),
         dma((2,)),
-        dma((n,)),
-        dma((n,)),
+        dma((3, n)),
+        dma((3, n)),
         dma((n,)),
         dma((n,)),
         dma((n,)),
@@ -490,19 +555,20 @@
         dma((n,)),
         dma((n,)),
     ]
-    return pl.pallas_call(
+    outs = (
+        jax.ShapeDtypeStruct(tokens.shape, tokens.dtype),
+        jax.ShapeDtypeStruct(state.shape, state.dtype),
+    )
+    result, new_state = pl.pallas_call(
         functools.partial(layer_kernel, n),
-        out_shape=(
-            jax.ShapeDtypeStruct(tokens.shape, tokens.dtype),
-            jax.ShapeDtypeStruct(state.shape, state.dtype),
-        ),
+        out_shape=(vmem(tokens.shape, tokens.dtype), vmem(state.shape, state.dtype)),
         in_specs=[anywhere] * 3
         + [pl.BlockSpec(memory_space=pltpu.SMEM)]
         + [anywhere] * 8,
-        out_specs=(anywhere, anywhere),
+        out_specs=(inside, inside),
         scratch_shapes=scratch,
         compiler_params=pltpu.CompilerParams(
-            collective_id=0, has_side_effects=True, vmem_limit_bytes=60 * 1024 * 1024
+            collective_id=0, has_side_effects=True, vmem_limit_bytes=64700000
         ),
         name="retention_layer",
     )(
@@ -519,6 +585,15 @@
         w_down,
         state,
     )
+    return pl.pallas_call(
+        write_out,
+        out_shape=outs,
+        in_specs=[inside, inside],
+        out_specs=(anywhere, anywhere),
+        scratch_shapes=[dma((2,))],
+        compiler_params=pltpu.CompilerParams(vmem_limit_bytes=4 * 1024 * 1024),
+        name="write_out",
+    )(result, new_state)
 
 
 def device_program(n, n_tp, tokens, *rest):
@@ -537,7 +612,7 @@
         and seqs % 8 == 0
         and 2 * seqs <= 128
     )
-    if n_tp == 2 and fits and aligned:
+    if n_tp == 2 and n % 2 == 0 and fits and aligned:
         return fused_device(n, tokens, *rest)
     return per_device(tokens, *rest)
 

time: 43.2 us -> 34.3 us (0.79)
  local copies, waits for them, and re-layouts: 4.53 us -> 0 us
  Pallas kernels: 37.8 us -> 33.5 us
    unnamed x2 -> x0, local copies, waits for them, and re-layouts: 4.53 us -> none
    pallas_call x1 -> x2, Pallas kernels: 37.8 us -> 33.5 us  [the longest x1 32.1 us: fused_device(): pl.pallas_call(functools.partial(layer_kernel, n), out_shape=(vmem(tokens...]
where the time goes in v2:
time: 34.3 us; the launch traced here: 34.1 us
  Pallas kernels  33.5 us (98%)
  between operations  0.64 us (2%)
    pallas_call x1, Pallas kernels, fused_device(): pl.pallas_call(functools.partial(layer_kernel, n), out_shape=(vmem(tokens...  32.1 us
    pallas_call x1, Pallas kernels, fused_device(): pl.pallas_call(write_out, out_shape=outs, in_specs=[inside, inside], out_...  1.34 us

profile of v2, /device:TPU:0, one launch (start us, length us, event | category | flops | bytes accessed | tf_op | source)
XLA Modules:
  0.0 34.1 jit_solution(6084556331696699289)
XLA Ops:
  0.6 32.1 %retention_layer.1 = (bf16[32,512]{1,0:T(8,128)(2,1)S(1)}, f32[8,8,64,128]{3,2,1,0:T(8,128)S(1)}) custom-call(bf16[32,512]{1,0:T(8,128)(2,1)} %tokens_hbm.1, f32[1,4096]{1,0:T(1,128)} %bitcast.2, f32[1,4096]{1,0:T(1,128)} %bitcast.3, f32[16]{0:T(128)} %rate_ref.1, bf16[1024,512]{1,0:T(8,128)(2,1)} %wq_hbm.1, bf16[1024,512]{1,0:T(8,128)(2,1)} %wk_hbm.1, ...), custom_call_target="tpu_custom_call" | custom-call | tf_op jit(solution)/shard_map/retention_layer/pallas_call | solution.py:562
  32.8 1.3 %write_out.1 = (bf16[32,512]{1,0:T(8,128)(2,1)}, f32[8,8,64,128]{3,2,1,0:T(8,128)}) custom-call(bf16[32,512]{1,0:T(8,128)(2,1)S(1)} %get-tuple-element.4.res, f32[8,8,64,128]{3,2,1,0:T(8,128)S(1)} %get-tuple-element.5.st), custom_call_target="tpu_custom_call" | custom-call | tf_op jit(solution)/shard_map/write_out/pallas_call | solution.py:588

commit v3 on v2

--- a/solution.py
+++ b/solution.py
@@ -386,9 +386,9 @@
     resid[me] = (
         tok[...].astype(F32) + (own_mix.astype(F32) + mix_in[...].astype(F32))
     ).astype(BF)
-    for i, k in enumerate(far):
+    sent.append(send(resid.at[me], resid.at[me], res_send.at[n - 1], res_recv.at[me], kv, other))
+    for i, k in enumerate(near):
         sent.append(send(resid.at[me], resid.at[me], res_send.at[i], res_recv.at[me], k, tp))
-    sent.append(send(resid.at[me], resid.at[me], res_send.at[n - 1], res_recv.at[me], kv, other))
     loads[8].wait()
 
     def up_step(j, so_far):

time: 34.3 us -> 33.4 us (0.974)
  Pallas kernels: 33.5 us -> 32.6 us
    pallas_call x1, Pallas kernels: 32.1 us -> 31.2 us  [fused_device(): pl.pallas_call(functools.partial(layer_kernel, n), out_shape=(vmem(tokens...]
where the time goes in v3:
time: 33.4 us; the launch traced here: 33.2 us
  Pallas kernels  32.6 us (98%)
  between operations  0.64 us (2%)
    pallas_call x1, Pallas kernels, fused_device(): pl.pallas_call(functools.partial(layer_kernel, n), out_shape=(vmem(tokens...  31.2 us
    pallas_call x1, Pallas kernels, fused_device(): pl.pallas_call(write_out, out_shape=outs, in_specs=[inside, inside], out_...  1.34 us

profile of v3, /device:TPU:0, one launch (start us, length us, event | category | flops | bytes accessed | tf_op | source)
XLA Modules:
  0.0 33.2 jit_solution(457480481302727362)
XLA Ops:
  0.6 31.2 %retention_layer.1 = (bf16[32,512]{1,0:T(8,128)(2,1)S(1)}, f32[8,8,64,128]{3,2,1,0:T(8,128)S(1)}) custom-call(bf16[32,512]{1,0:T(8,128)(2,1)} %tokens_hbm.1, f32[1,4096]{1,0:T(1,128)} %bitcast.2, f32[1,4096]{1,0:T(1,128)} %bitcast.3, f32[16]{0:T(128)} %rate_ref.1, bf16[1024,512]{1,0:T(8,128)(2,1)} %wq_hbm.1, bf16[1024,512]{1,0:T(8,128)(2,1)} %wk_hbm.1, ...), custom_call_target="tpu_custom_call" | custom-call | tf_op jit(solution)/shard_map/retention_layer/pallas_call | solution.py:562
  31.9 1.3 %write_out.1 = (bf16[32,512]{1,0:T(8,128)(2,1)}, f32[8,8,64,128]{3,2,1,0:T(8,128)}) custom-call(bf16[32,512]{1,0:T(8,128)(2,1)S(1)} %get-tuple-element.4.res, f32[8,8,64,128]{3,2,1,0:T(8,128)S(1)} %get-tuple-element.5.st), custom_call_target="tpu_custom_call" | custom-call | tf_op jit(solution)/shard_map/write_out/pallas_call | solution.py:588
